TPU v7x, 256 devices: a whole 4x4x8 slice. The times are simulated.
256 devices in a mesh: ep: 16 (over y, x), tp: 16 (over z, core).
Axes of the slice: x: 4, y: 4, z: 8, core: 2. Of those that a mesh axis runs over, the one named last changes fastest.
Arguments:
- queries: bfloat16 [16384, 1024], P('ep', 'tp'), may hold values from -8 to 8
- keys: bfloat16 [16384, 256], P('ep'), may hold values from -8 to 8
- values: bfloat16 [16384, 256], P('ep'), may hold values from -6 to 6
- query_gain: float32 [64], replicated, may hold values from 1 to 10
- key_gain: float32 [64], replicated, may hold values from 1 to 10
- moe_input: bfloat16 [12288, 2048], P(('ep', 'tp')), may hold values from -6 to 6
- expert_ids: int32 [12288, 2], P('ep'), may hold values from 0 to 15, all different within a row; in each aligned block of 48 rows (0 to 47, 48 to 95, ...) at most 7 rows name the same one
- route_weight: float32 [12288, 2], P('ep'), may hold values from 0.2 to 1
- gate_weight: bfloat16 [16, 2048, 7168], P('ep', None, 'tp'), may hold values from -0.125 to 0.125
- up_weight: bfloat16 [16, 2048, 7168], P('ep', None, 'tp'), may hold values from -0.125 to 0.125
- down_weight: bfloat16 [16, 7168, 2048], P('ep', 'tp'), may hold values from -0.0625 to 0.0625
- output_gain: float32 [2048], replicated, may hold values from 0.1 to 1.9
Outputs:
- attended: bfloat16 [16384, 1024], P('ep', 'tp')
- moe_output: bfloat16 [12288, 2048], P(('ep', 'tp'))
Inputs may be any that keep to these rules, and one draw needn't show every extreme that they name: `expert_ids`: the 2 experts of a token differ. In the rows of one device (aligned blocks of 48 tokens) no expert is named by more than 7 tokens, and in every draw some expert is named by exactly 7 tokens of some device.
All inputs are finite; a program needn't handle non-finite values.
Results may differ from a plain program's by a relative error of at most 0.0085.
The roundings to bfloat16 on the way count: a program that leaves them out, or rounds other values in their place, can miss the bound.
Values may be sent and summed in bfloat16 or wider, within the bound.
A program may use at most 128 MiB of HBM per device.

v0:
```python
import math
import jax
import jax.numpy as jnp
from jax import lax
from jax.sharding import Mesh
from jax.sharding import PartitionSpec as P

QH = 16
KV = 4
GRID_W = 64
TP = ("tp_0", "tp_1")
EP_TP = ("ep", "tp_0", "tp_1")
rope_theta = 10000.0
rms_epsilon = 1e-06
norm_epsilon = 1e-05
residual_scale = 1.4142135623730951


def side_by_side(arrays, axis, dim, along):
    ends, at = ([], 0)
    for a in arrays[:-1]:
        at += a.shape[along]
        ends.append(at)
    both = jnp.concatenate(arrays, axis=along)
    return tuple(jnp.split(lax.all_gather(both, axis, axis=dim, tiled=True), ends, axis=along))


def sum_by_axis(terms, axes):
    subtotal = terms.astype(jnp.bfloat16)
    for axis in axes:
        subtotal = lax.psum_scatter(subtotal, axis, scatter_dimension=0, tiled=True)
    return subtotal.astype(jnp.float32)


def unit_heads(heads, gain_vector):
    squares = jnp.mean(heads * heads, axis=-1, keepdims=True)
    return heads * lax.rsqrt(squares + rms_epsilon) * gain_vector


def rotate_grid(heads, first_position, grid_width):
    head_size = heads.shape[-1]
    pair_count = head_size // 4
    position = first_position + jnp.arange(heads.shape[1], dtype=jnp.int32)
    grid_row = (position // grid_width).astype(jnp.float32)
    grid_col = (position % grid_width).astype(jnp.float32)
    inverse = rope_theta ** (-jnp.arange(pair_count, dtype=jnp.float32) / pair_count)
    angles = jnp.concatenate([grid_row[:, None] * inverse, grid_col[:, None] * inverse], axis=-1)
    cosines = jnp.cos(angles)
    sines = jnp.sin(angles)
    half_size = head_size // 2
    first_half = heads[..., :half_size]
    second_half = heads[..., half_size:]
    return jnp.concatenate(
        [first_half * cosines - second_half * sines, second_half * cosines + first_half * sines],
        axis=-1,
    )


def place_rank(choices, expert_count):
    matches = (choices[..., None] == jnp.arange(expert_count, dtype=jnp.int32)).astype(jnp.int32)
    earlier = jnp.cumsum(matches, axis=1) - matches
    return jnp.sum(earlier * matches, axis=-1)


def shards(
    queries,
    keys,
    values,
    query_gain,
    key_gain,
    moe_input,
    expert_ids,
    route_weight,
    gate_weight,
    up_weight,
    down_weight,
    output_gain,
):
    seg_rows = queries.shape[0]
    head_size = query_gain.shape[0]
    local_heads = queries.shape[1] // head_size
    offset = lax.axis_index("ep") * seg_rows
    key_head = lax.axis_index(TP) * local_heads // (QH // KV)
    key_cols = lax.dynamic_slice_in_dim(keys, key_head * head_size, head_size, 1)
    value_cols = lax.dynamic_slice_in_dim(values, key_head * head_size, head_size, 1)
    query_heads = (
        queries.reshape(seg_rows, local_heads, head_size).transpose(1, 0, 2).astype(jnp.float32)
    )
    rotated_queries = rotate_grid(unit_heads(query_heads, query_gain), offset, GRID_W).astype(
        jnp.bfloat16
    )
    key_heads = key_cols.astype(jnp.float32)[None]
    rotated_keys = rotate_grid(unit_heads(key_heads, key_gain), offset, GRID_W)[0].astype(
        jnp.bfloat16
    )
    score_scale = head_size ** (-0.5)
    initial = (
        jnp.full((local_heads, seg_rows), -jnp.inf, jnp.float32),
        jnp.zeros((local_heads, seg_rows), jnp.float32),
        jnp.zeros((local_heads, head_size, seg_rows), jnp.float32),
    )
    key_piece, value_piece = side_by_side((rotated_keys, value_cols), "ep", 0, 1)
    piece_rows = key_piece.shape[0]
    block_rows = math.gcd(piece_rows, 1024)
    key_blocks = key_piece.reshape(piece_rows // block_rows, block_rows, head_size)
    value_blocks = value_piece.reshape(piece_rows // block_rows, block_rows, head_size)

    def sweep(state_now, blocks):
        running_max, row_total, summed = state_now
        key_block, value_block = blocks
        scores = (
            jnp.einsum(
                "hqd,kd->hqk", rotated_queries, key_block, preferred_element_type=jnp.float32
            )
            * score_scale
        )
        new_max = jnp.maximum(running_max, jnp.max(scores, axis=-1))
        shrink = jnp.exp(running_max - new_max)
        weights = jnp.exp(scores - new_max[..., None])
        row_total = row_total * shrink + jnp.sum(weights, axis=-1)
        added = jnp.einsum(
            "hqk,kd->hdq",
            weights.astype(jnp.bfloat16),
            value_block,
            preferred_element_type=jnp.float32,
        )
        summed = summed * shrink[:, None, :] + added
        return ((new_max, row_total, summed), None)

    result, ignored = lax.scan(sweep, initial, (key_blocks, value_blocks))
    row_max, row_total, summed = result
    attended = (
        (summed / row_total[:, None, :])
        .transpose(2, 0, 1)
        .reshape(seg_rows, local_heads * head_size)
        .astype(jnp.bfloat16)
    )
    tok_rows = moe_input.shape[0]
    model_width = moe_input.shape[1]
    top_count = expert_ids.shape[1]
    experts = lax.axis_size("ep")
    capacity = max(2, tok_rows * top_count * 5 // (4 * experts))
    column_index = lax.axis_index(TP)
    own_ids = lax.dynamic_slice_in_dim(expert_ids, column_index * tok_rows, tok_rows, 0).reshape(-1)
    own_weights = lax.dynamic_slice_in_dim(route_weight, column_index * tok_rows, tok_rows, 0)
    own_rank = place_rank(own_ids[None], experts)[0]
    own_slots = own_ids * capacity + own_rank
    token_of = jnp.arange(tok_rows * top_count, dtype=jnp.int32) // top_count
    sources = jnp.full((experts * capacity,), tok_rows, jnp.int32).at[own_slots].set(token_of)
    outgoing = jnp.take(moe_input, sources, axis=0, mode="fill", fill_value=0)
    arrived = lax.all_to_all(
        outgoing.reshape(experts, capacity, model_width),
        "ep",
        split_axis=0,
        concat_axis=0,
        tiled=True,
    )
    shard_piece = lax.all_gather(arrived.reshape(-1, model_width), TP, axis=0, tiled=True)
    gate_part = jnp.dot(shard_piece, gate_weight[0], preferred_element_type=jnp.float32)
    up_part = jnp.dot(shard_piece, up_weight[0], preferred_element_type=jnp.float32)
    hidden = (jax.nn.silu(gate_part) * up_part).astype(jnp.bfloat16)
    expert_out = sum_by_axis(
        jnp.dot(hidden, down_weight[0], preferred_element_type=jnp.float32), TP
    ).astype(jnp.bfloat16)
    returned = lax.all_to_all(
        expert_out.reshape(experts, capacity, model_width),
        "ep",
        split_axis=0,
        concat_axis=0,
        tiled=True,
    )
    picked = jnp.take(returned.reshape(experts * capacity, model_width), own_slots, axis=0)
    picked = picked.reshape(tok_rows, top_count, model_width).astype(jnp.float32)
    mixed = residual_scale * moe_input.astype(jnp.float32) + jnp.sum(
        own_weights[:, :, None] * picked, axis=1
    )
    average = jnp.mean(mixed, axis=-1, keepdims=True)
    centered = mixed - average
    variance = jnp.mean(centered * centered, axis=-1, keepdims=True)
    moe_output = (centered * lax.rsqrt(variance + norm_epsilon) * output_gain).astype(jnp.bfloat16)
    return (attended, moe_output)


def solution(mesh):
    split = Mesh(mesh.devices.reshape(mesh.shape["ep"], 8, 2), ("ep", "tp_0", "tp_1"))
    return jax.shard_map(
        shards,
        mesh=split,
        in_specs=(
            P("ep", TP),
            P("ep", None),
            P("ep", None),
            P(),
            P(),
            P(EP_TP, None),
            P("ep", None),
            P("ep", None),
            P("ep", None, TP),
            P("ep", None, TP),
            P("ep", TP, None),
            P(),
        ),
        out_specs=(P("ep", TP), P(EP_TP, None)),
        check_vma=False,
    )
```

profile of v0, /device:TPU:1, one launch (start us, length us, event | category | flops | bytes accessed | tf_op | source)
XLA Modules:
  0.0 365.4 jit_solution(13836861877901142481)
XLA Ops:
  10.7 2.3 gather_fusion
  13.4 17.8 %all_to_all.10 = bf16[16,7,2048]{2,1,0:T(8,128)(2,1)S(1)} all-to-all(bf16[16,7,2048]{2,1,0:T(8,128)(2,1)S(1)} %broadcast_select_fusion.3), channel_id=1, replica_groups=mesh['ep'=16,'tp_0'=8,'tp_1'=2] {'ep'}, dimensions={0} | all-to-all | bytes 917504 | tf_op jit(solution)/shard_map/all_to_all | solution.py:151
  32.2 51.9 %all-gather.5.cloned.1.call-done = bf16[1792,2048]{1,0:T(8,128)(2,1)} async-done(((bf16[112,2048]{1,0:T(8,128)(2,1)}), bf16[1792,2048]{1,0:T(8,128)(2,1)}) %all-gather.5.cloned.1.call-update) | async-done | bytes 7340048 | tf_op jit(solution)/shard_map/all_gather | solution.py:158
  84.1 7.3 %fusion.24 = f32[1792,448]{0,1:T(8,128)S(1)} fusion(bf16[1792,2048]{1,0:T(8,128)(2,1)} %all-gather.5.cloned.1.call-done, bf16[1,2048,448]{1,2,0:T(8,128)(2,1)} %param.22), kind=kOutput, calls=%fused_computation.30 | convolution fusion | flops 3288334336 | bytes 12386304 | tf_op jit(solution)/shard_map/dot_general | solution.py:159
  91.4 3.8 %multiply_convert_fusion = bf16[1792,448]{0,1:T(8,128)(2,1)S(1)} fusion(f32[1792,448]{0,1:T(8,128)S(1)} %fusion.24, bf16[1792,2048]{1,0:T(8,128)(2,1)S(1)} %copy-done.8, bf16[1,2048,448]{1,2,0:T(8,128)(2,1)S(1)} %copy-done.9), kind=kOutput, calls=%fused_computation.27 | convolution fusion | flops 3293151232 | bytes 13991936 | tf_op jit(solution)/shard_map/dot_general | solution.py:160
  95.1 6.1 %convolution_convert_fusion = bf16[1792,2048]{1,0:T(8,128)(2,1)} fusion(bf16[1792,448]{0,1:T(8,128)(2,1)S(1)} %multiply_convert_fusion, bf16[1,448,2048]{2,1,0:T(8,128)(2,1)S(1)} %copy-done), kind=kOutput, calls=%fused_computation.26 | convolution fusion | flops 3292004352 | bytes 10780672 | tf_op jit(solution)/shard_map/dot_general | solution.py:163
  107.2 77.4 %reduce-scatter.3.cloned.1.call-done = bf16[224,2048]{1,0:T(8,128)(2,1)} async-done(((bf16[1792,2048]{1,0:T(8,128)(2,1)}), bf16[224,2048]{1,0:T(8,128)(2,1)}) %reduce-scatter.3.cloned.1.call-update) | async-done | bytes 917520 | tf_op jit(solution)/shard_map/reduce_scatter | solution.py:31
  184.7 4.7 %fusion.47 = (bf16[16384,64]{0,1:T(8,128)(2,1)}, bf16[16384,64]{0,1:T(8,128)(2,1)}) fusion(bf16[16384,128]{0,1:T(8,128)(2,1)} %all-gather.3.cloned.1.call-done), kind=kLoop, calls=%fused_computation.105 | loop fusion | bytes 8388608 | tf_op jit(solution)/shard_map/split | solution.py:25
  189.3 4.8 %copy.37 = bf16[16384,64]{1,0:T(8,128)(2,1)} copy(bf16[16384,64]{0,1:T(8,128)(2,1)} %get-tuple-element.101) | data formatting | bytes 4194304
  194.1 5.0 %copy.38 = bf16[16384,64]{1,0:T(8,128)(2,1)} copy(bf16[16384,64]{0,1:T(8,128)(2,1)} %get-tuple-element.100) | data formatting | bytes 4194304
  200.2 2.0 reshape.467
  202.1 6.2 %all-to-all-start.1 = ((bf16[16,7,2048]{2,1,0:T(8,128)(2,1)}), bf16[16,7,2048]{2,1,0:T(8,128)(2,1)S(1)}, u32[]{:S(2)}, u32[]{:S(2)}) async-start(bf16[16,7,2048]{2,1,0:T(8,128)(2,1)} %reshape.467), calls=%async_computation.3 | async-start | bytes 1048576 | tf_op jit(solution)/shard_map/all_to_all | solution.py:165
  208.4 144.6 %while.15 = (s32[]{:T(128)}, f32[1,1024]{1,0:T(1,128)S(1)}, f32[1,1024]{1,0:T(1,128)S(1)}, f32[1,64,1024]{2,1,0:T(8,128)S(1)}, bf16[16,1024,64]{2,1,0:T(8,128)(2...) while((s32[]{:T(128)}, f32[1,1024]{1,0:T(1,128)S(1)}, ...), condition=%wide.region_5.6_spmd.clone, body=%wide.region_2.5_spmd.clone.sunk | while | flops 277025792 | bytes 30605460 | solution.py:130
  208.4 3.8 %multiply_reduce_fusion.4 = (f32[1024]{0:T(1024)S(1)}, f32[1024,1024]{1,0:T(8,128)}) fusion(bf16[1,1024,64]{2,1,0:T(8,128)(2,1)S(1)} %get-tuple-element.188, bf16[16,1024,64]{2,1,0:T(8,128)(2,1)} %get-tuple-element.187, s32[]{:T(128)S(6)} %copy.45), kind=kOutput, calls=%fused_computation.4.clone.1 | convolution fusion | flops 136313856 | bytes 4591620 | tf_op jit(solution)/shard_map/while/body/eval_jaxpr/hqd,kd->hqk/dot_general | solution.py:112
  212.2 3.1 fusion.60
  215.6 1.8 fusion.62
  217.4 3.8 %multiply_reduce_fusion.4 = (f32[1024]{0:T(1024)S(1)}, f32[1024,1024]{1,0:T(8,128)}) fusion(bf16[1,1024,64]{2,1,0:T(8,128)(2,1)S(1)} %get-tuple-element.188, bf16[16,1024,64]{2,1,0:T(8,128)(2,1)} %get-tuple-element.187, s32[]{:T(128)S(6)} %copy.45), kind=kOutput, calls=%fused_computation.4.clone.1 | convolution fusion | flops 136313856 | bytes 4591620 | tf_op jit(solution)/shard_map/while/body/eval_jaxpr/hqd,kd->hqk/dot_general | solution.py:112
  221.2 3.1 fusion.60
  224.7 1.8 fusion.62
  226.5 3.8 %multiply_reduce_fusion.4 = (f32[1024]{0:T(1024)S(1)}, f32[1024,1024]{1,0:T(8,128)}) fusion(bf16[1,1024,64]{2,1,0:T(8,128)(2,1)S(1)} %get-tuple-element.188, bf16[16,1024,64]{2,1,0:T(8,128)(2,1)} %get-tuple-element.187, s32[]{:T(128)S(6)} %copy.45), kind=kOutput, calls=%fused_computation.4.clone.1 | convolution fusion | flops 136313856 | bytes 4591620 | tf_op jit(solution)/shard_map/while/body/eval_jaxpr/hqd,kd->hqk/dot_general | solution.py:112
  230.3 3.1 fusion.60
  235.5 3.8 %multiply_reduce_fusion.4 = (f32[1024]{0:T(1024)S(1)}, f32[1024,1024]{1,0:T(8,128)}) fusion(bf16[1,1024,64]{2,1,0:T(8,128)(2,1)S(1)} %get-tuple-element.188, bf16[16,1024,64]{2,1,0:T(8,128)(2,1)} %get-tuple-element.187, s32[]{:T(128)S(6)} %copy.45), kind=kOutput, calls=%fused_computation.4.clone.1 | convolution fusion | flops 136313856 | bytes 4591620 | tf_op jit(solution)/shard_map/while/body/eval_jaxpr/hqd,kd->hqk/dot_general | solution.py:112
  239.3 3.1 fusion.60
  244.5 3.8 %multiply_reduce_fusion.4 = (f32[1024]{0:T(1024)S(1)}, f32[1024,1024]{1,0:T(8,128)}) fusion(bf16[1,1024,64]{2,1,0:T(8,128)(2,1)S(1)} %get-tuple-element.188, bf16[16,1024,64]{2,1,0:T(8,128)(2,1)} %get-tuple-element.187, s32[]{:T(128)S(6)} %copy.45), kind=kOutput, calls=%fused_computation.4.clone.1 | convolution fusion | flops 136313856 | bytes 4591620 | tf_op jit(solution)/shard_map/while/body/eval_jaxpr/hqd,kd->hqk/dot_general | solution.py:112
  248.3 3.1 fusion.60
  253.6 3.8 %multiply_reduce_fusion.4 = (f32[1024]{0:T(1024)S(1)}, f32[1024,1024]{1,0:T(8,128)}) fusion(bf16[1,1024,64]{2,1,0:T(8,128)(2,1)S(1)} %get-tuple-element.188, bf16[16,1024,64]{2,1,0:T(8,128)(2,1)} %get-tuple-element.187, s32[]{:T(128)S(6)} %copy.45), kind=kOutput, calls=%fused_computation.4.clone.1 | convolution fusion | flops 136313856 | bytes 4591620 | tf_op jit(solution)/shard_map/while/body/eval_jaxpr/hqd,kd->hqk/dot_general | solution.py:112
  257.4 3.1 fusion.60
  262.6 3.8 %multiply_reduce_fusion.4 = (f32[1024]{0:T(1024)S(1)}, f32[1024,1024]{1,0:T(8,128)}) fusion(bf16[1,1024,64]{2,1,0:T(8,128)(2,1)S(1)} %get-tuple-element.188, bf16[16,1024,64]{2,1,0:T(8,128)(2,1)} %get-tuple-element.187, s32[]{:T(128)S(6)} %copy.45), kind=kOutput, calls=%fused_computation.4.clone.1 | convolution fusion | flops 136313856 | bytes 4591620 | tf_op jit(solution)/shard_map/while/body/eval_jaxpr/hqd,kd->hqk/dot_general | solution.py:112
  266.4 3.1 fusion.60
  271.7 3.8 %multiply_reduce_fusion.4 = (f32[1024]{0:T(1024)S(1)}, f32[1024,1024]{1,0:T(8,128)}) fusion(bf16[1,1024,64]{2,1,0:T(8,128)(2,1)S(1)} %get-tuple-element.188, bf16[16,1024,64]{2,1,0:T(8,128)(2,1)} %get-tuple-element.187, s32[]{:T(128)S(6)} %copy.45), kind=kOutput, calls=%fused_computation.4.clone.1 | convolution fusion | flops 136313856 | bytes 4591620 | tf_op jit(solution)/shard_map/while/body/eval_jaxpr/hqd,kd->hqk/dot_general | solution.py:112
  275.4 3.1 fusion.60
  280.7 3.8 %multiply_reduce_fusion.4 = (f32[1024]{0:T(1024)S(1)}, f32[1024,1024]{1,0:T(8,128)}) fusion(bf16[1,1024,64]{2,1,0:T(8,128)(2,1)S(1)} %get-tuple-element.188, bf16[16,1024,64]{2,1,0:T(8,128)(2,1)} %get-tuple-element.187, s32[]{:T(128)S(6)} %copy.45), kind=kOutput, calls=%fused_computation.4.clone.1 | convolution fusion | flops 136313856 | bytes 4591620 | tf_op jit(solution)/shard_map/while/body/eval_jaxpr/hqd,kd->hqk/dot_general | solution.py:112
  284.5 3.1 fusion.60
  289.7 3.8 %multiply_reduce_fusion.4 = (f32[1024]{0:T(1024)S(1)}, f32[1024,1024]{1,0:T(8,128)}) fusion(bf16[1,1024,64]{2,1,0:T(8,128)(2,1)S(1)} %get-tuple-element.188, bf16[16,1024,64]{2,1,0:T(8,128)(2,1)} %get-tuple-element.187, s32[]{:T(128)S(6)} %copy.45), kind=kOutput, calls=%fused_computation.4.clone.1 | convolution fusion | flops 136313856 | bytes 4591620 | tf_op jit(solution)/shard_map/while/body/eval_jaxpr/hqd,kd->hqk/dot_general | solution.py:112
  293.5 3.1 fusion.60
  298.8 3.8 %multiply_reduce_fusion.4 = (f32[1024]{0:T(1024)S(1)}, f32[1024,1024]{1,0:T(8,128)}) fusion(bf16[1,1024,64]{2,1,0:T(8,128)(2,1)S(1)} %get-tuple-element.188, bf16[16,1024,64]{2,1,0:T(8,128)(2,1)} %get-tuple-element.187, s32[]{:T(128)S(6)} %copy.45), kind=kOutput, calls=%fused_computation.4.clone.1 | convolution fusion | flops 136313856 | bytes 4591620 | tf_op jit(solution)/shard_map/while/body/eval_jaxpr/hqd,kd->hqk/dot_general | solution.py:112
  302.5 3.1 fusion.60
  307.8 3.8 %multiply_reduce_fusion.4 = (f32[1024]{0:T(1024)S(1)}, f32[1024,1024]{1,0:T(8,128)}) fusion(bf16[1,1024,64]{2,1,0:T(8,128)(2,1)S(1)} %get-tuple-element.188, bf16[16,1024,64]{2,1,0:T(8,128)(2,1)} %get-tuple-element.187, s32[]{:T(128)S(6)} %copy.45), kind=kOutput, calls=%fused_computation.4.clone.1 | convolution fusion | flops 136313856 | bytes 4591620 | tf_op jit(solution)/shard_map/while/body/eval_jaxpr/hqd,kd->hqk/dot_general | solution.py:112
  311.6 3.1 fusion.60
  316.8 3.8 %multiply_reduce_fusion.4 = (f32[1024]{0:T(1024)S(1)}, f32[1024,1024]{1,0:T(8,128)}) fusion(bf16[1,1024,64]{2,1,0:T(8,128)(2,1)S(1)} %get-tuple-element.188, bf16[16,1024,64]{2,1,0:T(8,128)(2,1)} %get-tuple-element.187, s32[]{:T(128)S(6)} %copy.45), kind=kOutput, calls=%fused_computation.4.clone.1 | convolution fusion | flops 136313856 | bytes 4591620 | tf_op jit(solution)/shard_map/while/body/eval_jaxpr/hqd,kd->hqk/dot_general | solution.py:112
  320.6 3.1 fusion.60
  325.9 3.8 %multiply_reduce_fusion.4 = (f32[1024]{0:T(1024)S(1)}, f32[1024,1024]{1,0:T(8,128)}) fusion(bf16[1,1024,64]{2,1,0:T(8,128)(2,1)S(1)} %get-tuple-element.188, bf16[16,1024,64]{2,1,0:T(8,128)(2,1)} %get-tuple-element.187, s32[]{:T(128)S(6)} %copy.45), kind=kOutput, calls=%fused_computation.4.clone.1 | convolution fusion | flops 136313856 | bytes 4591620 | tf_op jit(solution)/shard_map/while/body/eval_jaxpr/hqd,kd->hqk/dot_general | solution.py:112
  329.6 3.1 fusion.60
  334.9 3.8 %multiply_reduce_fusion.4 = (f32[1024]{0:T(1024)S(1)}, f32[1024,1024]{1,0:T(8,128)}) fusion(bf16[1,1024,64]{2,1,0:T(8,128)(2,1)S(1)} %get-tuple-element.188, bf16[16,1024,64]{2,1,0:T(8,128)(2,1)} %get-tuple-element.187, s32[]{:T(128)S(6)} %copy.45), kind=kOutput, calls=%fused_computation.4.clone.1 | convolution fusion | flops 136313856 | bytes 4591620 | tf_op jit(solution)/shard_map/while/body/eval_jaxpr/hqd,kd->hqk/dot_general | solution.py:112
  338.7 3.1 fusion.60
  343.9 3.8 %multiply_reduce_fusion.4 = (f32[1024]{0:T(1024)S(1)}, f32[1024,1024]{1,0:T(8,128)}) fusion(bf16[1,1024,64]{2,1,0:T(8,128)(2,1)S(1)} %get-tuple-element.188, bf16[16,1024,64]{2,1,0:T(8,128)(2,1)} %get-tuple-element.187, s32[]{:T(128)S(6)} %copy.45), kind=kOutput, calls=%fused_computation.4.clone.1 | convolution fusion | flops 136313856 | bytes 4591620 | tf_op jit(solution)/shard_map/while/body/eval_jaxpr/hqd,kd->hqk/dot_general | solution.py:112
  347.7 3.1 fusion.60
  354.9 2.0 multiply_reduce_fusion.1
  (177 shorter events, 44.9 us)
Async XLA Ops:
  8.0 87.1 %copy-start = (bf16[1,448,2048]{2,1,0:T(8,128)(2,1)S(1)}, bf16[1,448,2048]{2,1,0:T(8,128)(2,1)}, u32[]{:S(2)}) copy-start(bf16[1,448,2048]{2,1,0:T(8,128)(2,1)} %param.24) | copy-start | bytes 5505028
  8.0 76.1 %all-gather.5.cloned.1.call-start = ((), (), s32[]{:S(2)}) async-start(), calls=%async_computation.5 | async-start | bytes 7798784 | tf_op jit(solution)/shard_map/all_gather | solution.py:158
  32.1 152.5 %reduce-scatter.3.cloned.1.call-start = ((), (), s32[]{:S(2)}) async-start(), calls=%async_computation.6 | async-start | bytes 8257536 | tf_op jit(solution)/shard_map/reduce_scatter | solution.py:31
  84.1 7.3 %copy-start.8 = (bf16[1792,2048]{1,0:T(8,128)(2,1)S(1)}, bf16[1792,2048]{1,0:T(8,128)(2,1)}, u32[]{:S(2)}) copy-start(bf16[1792,2048]{1,0:T(8,128)(2,1)} %all-gather.5.cloned.1.call-done) | copy-start | bytes 22020100
  84.1 7.3 %copy-start.9 = (bf16[1,2048,448]{1,2,0:T(8,128)(2,1)S(1)}, bf16[1,2048,448]{1,2,0:T(8,128)(2,1)}, u32[]{:S(2)}) copy-start(bf16[1,2048,448]{1,2,0:T(8,128)(2,1)} %param.23) | copy-start | bytes 5505028
  101.3 1.0 copy-start.4
  101.3 2.5 copy-start.3
  101.3 2.7 copy-start.6
  101.3 2.8 copy-start.7
  101.3 83.3 %all-gather.3.cloned.1.call-start = ((), (), s32[]{:S(2)}) async-start(), calls=%async_computation.4 | async-start | bytes 4456448 | tf_op jit(solution)/shard_map/all_gather | solution.py:25
  105.5 94.7 %reduce-scatter.5.cloned.1.call-start = ((), (), s32[]{:S(2)}) async-start(), calls=%async_computation.7 | async-start | bytes 1376256 | tf_op jit(solution)/shard_map/reduce_scatter | solution.py:31
  202.1 151.5 %all-to-all-start.1 = ((bf16[16,7,2048]{2,1,0:T(8,128)(2,1)}), bf16[16,7,2048]{2,1,0:T(8,128)(2,1)S(1)}, u32[]{:S(2)}, u32[]{:S(2)}) async-start(bf16[16,7,2048]{2,1,0:T(8,128)(2,1)} %reshape.467), calls=%async_computation.3 | async-start | bytes 1048576 | tf_op jit(solution)/shard_map/all_to_all | solution.py:165
  212.2 3.4 copy-start.1
  221.2 3.4 copy-start.1
  230.2 3.4 copy-start.1
  239.3 3.4 copy-start.1
  248.3 3.4 copy-start.1
  257.3 3.4 copy-start.1
  266.4 3.4 copy-start.1
  275.4 3.4 copy-start.1
  284.5 3.4 copy-start.1
  293.5 3.4 copy-start.1
  302.5 3.4 copy-start.1
  311.6 3.4 copy-start.1
  320.6 3.4 copy-start.1
  329.6 3.4 copy-start.1
  338.7 3.4 copy-start.1
  347.7 3.4 copy-start.1
  353.0 4.0 %copy-start.2 = (bf16[48,2048]{1,0:T(8,128)(2,1)S(1)}, bf16[48,2048]{1,0:T(8,128)(2,1)}, u32[]{:S(2)}) copy-start(bf16[48,2048]{1,0:T(8,128)(2,1)} %param.19) | copy-start | bytes 589828
  353.0 4.4 %copy-start.5 = (f32[2048]{0:T(1024)S(1)}, f32[2048]{0:T(1024)}, u32[]{:S(2)}) copy-start(f32[2048]{0:T(1024)} %param.25) | copy-start | bytes 24580
Sparse Core Ops, SparseCore 0:
  32.3 51.7 all-gather.4
  101.4 83.1 reduce-scatter.2
  187.1 13.0 reduce-scatter.4
Sparse Core Ops, SparseCore 1:
  105.6 54.1 all-gather.2
where the time goes:
time: 367 us; the launch traced here: 365 us
  waiting for transfers between devices  130 us (35%)
  matrix products  106 us (29%)
  other arithmetic  56.6 us (15%)
  local copies, waits for them, and re-layouts  31.5 us (9%)
  blocking collectives  17.8 us (5%)
  between operations  15.6 us (4%)
  starting transfers between devices  6.59 us (2%)
    reduce_scatter x2, waiting for transfers between devices, sum_by_axis(): subtotal = lax.psum_scatter(subtotal, axis, scatter_dimension=0, tiled=True)  78.5 us
    dot_general x16, matrix products, sweep(): jnp.einsum('hqd,kd->hqk', rotated_queries, key_block, preferred_element_t...  60.3 us
    all_gather x1, waiting for transfers between devices, shards(): lax.all_gather(arrived.reshape(-1, model_width), TP, axis=0, tiled=True)  51.9 us
    reduce_sum x16, other arithmetic, sweep(): row_total = row_total * shrink + jnp.sum(weights, axis=-1)  49.1 us
    dot_general x16, matrix products, sweep(): jnp.einsum('hqk,kd->hdq', weights.astype(jnp.bfloat16), value_block, pref...  28.8 us
    all_to_all x1, blocking collectives, shards(): lax.all_to_all(outgoing.reshape(experts, capacity, model_width), 'ep', sp...  17.8 us
    unnamed x23, local copies, waits for them, and re-layouts  11.2 us
  transfers between devices with their start and end apart: 5, of which 3 were waited for; matrix products, arithmetic and copies ran while one was open for 43% of the time, Pallas kernels for 0%

commit v1 on v0

--- a/solution.py
+++ b/solution.py
@@ -155,7 +155,16 @@
         concat_axis=0,
         tiled=True,
     )
-    shard_piece = lax.all_gather(arrived.reshape(-1, model_width), TP, axis=0, tiled=True)
+    name_streams = lambda u, peer_axis: jnp.concatenate(
+        jax.lax.all_to_all(
+            jnp.stack(jax.lax.axis_size(peer_axis) * [u], 0),
+            axis_name=peer_axis,
+            split_axis=0,
+            concat_axis=0,
+        ),
+        0,
+    )
+    shard_piece = name_streams(arrived.reshape(-1, model_width), TP)
     gate_part = jnp.dot(shard_piece, gate_weight[0], preferred_element_type=jnp.float32)
     up_part = jnp.dot(shard_piece, up_weight[0], preferred_element_type=jnp.float32)
     hidden = (jax.nn.silu(gate_part) * up_part).astype(jnp.bfloat16)

time: 367 us -> 480 us (1.31)
  blocking collectives: 17.8 us -> 192 us
  waiting for transfers between devices: 130 us -> 73.6 us
    all_to_all x0 -> x1, blocking collectives: none -> 174 us  [shards(): jax.lax.all_to_all(jnp.stack(jax.lax.axis_size(peer_axis) * [u], 0), axis...]
    all_gather x1 -> x0, waiting for transfers between devices: 51.9 us -> none  [shards(): lax.all_gather(arrived.reshape(-1, model_width), TP, axis=0, tiled=True)]
    reduce_scatter x2, waiting for transfers between devices: 78.5 us -> 73.5 us  [sum_by_axis(): subtotal = lax.psum_scatter(subtotal, axis, scatter_dimension=0, tiled=True)]
  transfers between devices with their start and end apart: 5 -> 4, of which waited for: 3 -> 2; matrix products, arithmetic and copies ran while one was open for 43% -> 33% of each run, Pallas kernels for 0% -> 0%
where the time goes in v1:
time: 480 us; the launch traced here: 479 us
  blocking collectives  192 us (40%)
  matrix products  102 us (21%)
  waiting for transfers between devices  73.6 us (15%)
  other arithmetic  56.6 us (12%)
  local copies, waits for them, and re-layouts  31.6 us (7%)
  between operations  15.9 us (3%)
  starting transfers between devices  6.56 us (1%)
    all_to_all x1, blocking collectives, shards(): jax.lax.all_to_all(jnp.stack(jax.lax.axis_size(peer_axis) * [u], 0), axis...  174 us
    reduce_scatter x2, waiting for transfers between devices, sum_by_axis(): subtotal = lax.psum_scatter(subtotal, axis, scatter_dimension=0, tiled=True)  73.5 us
    dot_general x16, matrix products, sweep(): jnp.einsum('hqd,kd->hqk', rotated_queries, key_block, preferred_element_t...  60.3 us
    reduce_sum x16, other arithmetic, sweep(): row_total = row_total * shrink + jnp.sum(weights, axis=-1)  49.1 us
    dot_general x16, matrix products, sweep(): jnp.einsum('hqk,kd->hdq', weights.astype(jnp.bfloat16), value_block, pref...  28.8 us
    all_to_all x1, blocking collectives, shards(): lax.all_to_all(outgoing.reshape(experts, capacity, model_width), 'ep', sp...  17.8 us
    unnamed x23, local copies, waits for them, and re-layouts  11 us
  transfers between devices with their start and end apart: 4, of which 2 were waited for; matrix products, arithmetic and copies ran while one was open for 33% of the time, Pallas kernels for 0%

profile of v1, /device:TPU:1, one launch (start us, length us, event | category | flops | bytes accessed | tf_op | source)
XLA Modules:
  0.0 478.9 jit_solution(5194624725411069759)
XLA Ops:
  10.7 2.3 gather_fusion
  13.4 17.8 %all_to_all.15 = bf16[16,7,2048]{2,1,0:T(8,128)(2,1)S(1)} all-to-all(bf16[16,7,2048]{2,1,0:T(8,128)(2,1)S(1)} %broadcast_select_fusion.3), channel_id=1, replica_groups=mesh['ep'=16,'tp_0'=8,'tp_1'=2] {'ep'}, dimensions={0} | all-to-all | bytes 917504 | tf_op jit(solution)/shard_map/all_to_all | solution.py:151
  32.3 173.7 %all_to_all.16 = bf16[16,112,2048]{2,1,0:T(8,128)(2,1)S(1)} all-to-all(bf16[16,112,2048]{2,1,0:T(8,128)(2,1)S(1)} %stack.3), channel_id=1, replica_groups=mesh['ep'=16,'tp_0'=8,'tp_1'=2] {'tp_0','tp_1'}, dimensions={0} | all-to-all | bytes 14680064 | tf_op jit(solution)/shard_map/all_to_all | solution.py:159
  206.0 3.5 fusion.24
  209.6 3.8 multiply_convert_fusion
  213.4 6.1 %convolution_convert_fusion = bf16[1792,2048]{1,0:T(8,128)(2,1)} fusion(bf16[1792,448]{0,1:T(8,128)(2,1)S(1)} %multiply_convert_fusion, bf16[1,448,2048]{2,1,0:T(8,128)(2,1)S(1)} %copy-done), kind=kOutput, calls=%fused_computation.26 | convolution fusion | flops 3292004352 | bytes 10780672 | tf_op jit(solution)/shard_map/dot_general | solution.py:172
  225.2 72.4 %reduce-scatter.3.cloned.1.call-done = bf16[224,2048]{1,0:T(8,128)(2,1)} async-done(((bf16[1792,2048]{1,0:T(8,128)(2,1)}), bf16[224,2048]{1,0:T(8,128)(2,1)}) %reduce-scatter.3.cloned.1.call-update) | async-done | bytes 917520 | tf_op jit(solution)/shard_map/reduce_scatter | solution.py:31
  297.6 4.7 fusion.47
  302.3 4.8 copy.37
  307.1 5.0 %copy.38 = bf16[16384,64]{1,0:T(8,128)(2,1)} copy(bf16[16384,64]{0,1:T(8,128)(2,1)} %get-tuple-element.100) | data formatting | bytes 4194304
  313.2 2.0 reshape.469
  315.1 6.3 %all-to-all-start.2 = ((bf16[16,7,2048]{2,1,0:T(8,128)(2,1)}), bf16[16,7,2048]{2,1,0:T(8,128)(2,1)S(1)}, u32[]{:S(2)}, u32[]{:S(2)}) async-start(bf16[16,7,2048]{2,1,0:T(8,128)(2,1)} %reshape.469), calls=%async_computation.4 | async-start | bytes 1048576 | tf_op jit(solution)/shard_map/all_to_all | solution.py:174
  321.4 144.8 %while.15 = (s32[]{:T(128)}, f32[1,1024]{1,0:T(1,128)S(1)}, f32[1,1024]{1,0:T(1,128)S(1)}, f32[1,64,1024]{2,1,0:T(8,128)S(1)}, bf16[16,1024,64]{2,1,0:T(8,128)(2...) while((s32[]{:T(128)}, f32[1,1024]{1,0:T(1,128)S(1)}, ...), condition=%wide.region_5.6_spmd.clone, body=%wide.region_2.5_spmd.clone.sunk | while | flops 277025792 | bytes 30606468 | solution.py:130
  321.4 3.8 multiply_reduce_fusion.4
  325.2 3.1 fusion.60
  328.6 1.8 fusion.62
  330.5 3.8 multiply_reduce_fusion.4
  334.3 3.1 fusion.60
  339.5 3.8 multiply_reduce_fusion.4
  343.3 3.1 fusion.60
  346.7 1.8 fusion.62
  348.6 3.8 multiply_reduce_fusion.4
  352.3 3.1 fusion.60
  357.6 3.8 multiply_reduce_fusion.4
  361.4 3.1 fusion.60
  366.7 3.8 multiply_reduce_fusion.4
  370.4 3.1 fusion.60
  375.7 3.8 multiply_reduce_fusion.4
  379.5 3.1 fusion.60
  384.8 3.8 multiply_reduce_fusion.4
  388.5 3.1 fusion.60
  393.8 3.8 multiply_reduce_fusion.4
  397.6 3.1 fusion.60
  402.9 3.8 multiply_reduce_fusion.4
  406.6 3.1 fusion.60
  411.9 3.8 multiply_reduce_fusion.4
  415.7 3.1 fusion.60
  421.0 3.8 multiply_reduce_fusion.4
  424.7 3.1 fusion.60
  430.0 3.8 multiply_reduce_fusion.4
  433.8 3.1 fusion.60
  439.1 3.8 multiply_reduce_fusion.4
  442.8 3.1 fusion.60
  448.1 3.8 multiply_reduce_fusion.4
  451.9 3.1 fusion.60
  457.2 3.8 multiply_reduce_fusion.4
  460.9 3.1 fusion.60
  468.2 2.0 multiply_reduce_fusion.1
  (176 shorter events, 45.1 us)
Async XLA Ops:
  8.0 205.4 %copy-start = (bf16[1,448,2048]{2,1,0:T(8,128)(2,1)S(1)}, bf16[1,448,2048]{2,1,0:T(8,128)(2,1)}, u32[]{:S(2)}) copy-start(bf16[1,448,2048]{2,1,0:T(8,128)(2,1)} %param.24) | copy-start | bytes 5505028
  8.0 289.6 %reduce-scatter.3.cloned.1.call-start = ((), (), s32[]{:S(2)}) async-start(), calls=%async_computation.6 | async-start | bytes 8257536 | tf_op jit(solution)/shard_map/reduce_scatter | solution.py:31
  32.3 173.7 %copy-start.8 = (bf16[1,2048,448]{1,2,0:T(8,128)(2,1)S(1)}, bf16[1,2048,448]{1,2,0:T(8,128)(2,1)}, u32[]{:S(2)}) copy-start(bf16[1,2048,448]{1,2,0:T(8,128)(2,1)} %param.22) | copy-start | bytes 5505028
  206.0 3.5 copy-start.9
  219.5 1.0 copy-start.4
  219.5 2.6 copy-start.3
  219.5 2.7 copy-start.6
  219.5 2.8 copy-start.7
  219.5 78.1 %all-gather.2.cloned.1.call-start = ((), (), s32[]{:S(2)}) async-start(), calls=%async_computation.5 | async-start | bytes 4456448 | tf_op jit(solution)/shard_map/all_gather | solution.py:25
  223.7 89.4 %reduce-scatter.5.cloned.1.call-start = ((), (), s32[]{:S(2)}) async-start(), calls=%async_computation.7 | async-start | bytes 1376256 | tf_op jit(solution)/shard_map/reduce_scatter | solution.py:31
  315.1 151.8 %all-to-all-start.2 = ((bf16[16,7,2048]{2,1,0:T(8,128)(2,1)}), bf16[16,7,2048]{2,1,0:T(8,128)(2,1)S(1)}, u32[]{:S(2)}, u32[]{:S(2)}) async-start(bf16[16,7,2048]{2,1,0:T(8,128)(2,1)} %reshape.469), calls=%async_computation.4 | async-start | bytes 1048576 | tf_op jit(solution)/shard_map/all_to_all | solution.py:174
  325.2 3.4 copy-start.1
  334.2 3.4 copy-start.1
  343.3 3.4 copy-start.1
  352.3 3.4 copy-start.1
  361.4 3.4 copy-start.1
  370.4 3.4 copy-start.1
  379.5 3.4 copy-start.1
  388.5 3.4 copy-start.1
  397.6 3.4 copy-start.1
  406.6 3.4 copy-start.1
  415.7 3.4 copy-start.1
  424.7 3.4 copy-start.1
  433.8 3.4 copy-start.1
  442.8 3.4 copy-start.1
  451.9 3.4 copy-start.1
  460.9 3.4 copy-start.1
  466.2 4.0 copy-start.2
  466.2 4.4 copy-start.5
Sparse Core Ops, SparseCore 0:
  219.7 77.8 reduce-scatter.2
  300.1 13.0 reduce-scatter.4
Sparse Core Ops, SparseCore 1:
  223.8 48.9 all-gather.1
